TPU v7x, 32 devices: a whole 2x2x4 slice. The times are simulated.
32 devices in a mesh: sp: 8 (over z, core), tp: 4 (over y, x).
Axes of the slice: x: 2, y: 2, z: 4, core: 2. Of those that a mesh axis runs over, the one named last changes fastest.
Arguments:
- receptance: bfloat16 [2048, 4096], P('sp', 'tp'), may hold values from -6 to 6
- key_vectors: bfloat16 [2048, 4096], P('sp', 'tp'), may hold values from -13 to 13
- value_vectors: bfloat16 [2048, 4096], P('sp', 'tp'), may hold values from -6 to 6
- decay_logits: bfloat16 [2048, 4096], P('sp', 'tp'), may hold values from -20 to 2
- rate_logits: bfloat16 [2048, 4096], P('sp', 'tp'), may hold values from -8 to 4
- gate_logits: bfloat16 [2048, 4096], P('sp', 'tp'), may hold values from -6 to 6
- group_gain: float32 [4096], P('tp'), may hold values from 0.1 to 1.9
- residual: bfloat16 [2048, 4096], P('sp', 'tp'), may hold values from -24 to 24
- mixer_out: bfloat16 [4096, 4096], P(None, 'tp'), may hold values from -0.09375 to 0.09375
- norm_gain: float32 [4096], P('tp'), may hold values from 0.1 to 1.9
- expert_ids: int32 [2048, 2], P('sp'), may hold values from 0 to 7, as said below
- route_weight: float32 [2048, 2], P('sp'), may hold values from 0.25 to 1
- expert_gate: bfloat16 [8, 4096, 1024], P('sp', 'tp'), may hold values from -0.09375 to 0.09375
- expert_up: bfloat16 [8, 4096, 1024], P('sp', 'tp'), may hold values from -0.09375 to 0.09375
- expert_down: bfloat16 [8, 1024, 4096], P('sp', None, 'tp'), may hold values from -0.1875 to 0.1875
Outputs:
- updated: bfloat16 [2048, 4096], P('sp', 'tp')
Inputs may be any that keep to these rules, and one draw needn't show every extreme that they name: `expert_ids`: the experts of a row are different and lie in one group of 2 consecutive experts. In the rows of one index of sp (aligned blocks of 256 rows) no expert is named by more than 128 rows, and in every such block some expert is named by exactly 128 rows.
All inputs are finite; a program needn't handle non-finite values.
Results may differ from a plain program's by a relative error of at most 0.013.
Values may be sent and summed in bfloat16 or wider, within the bound.
A program may use at most 128 MiB of HBM per device.

v0:
```python
import jax
import jax.numpy as jnp
from jax import lax
from jax.sharding import PartitionSpec as P

D = 4096
HEAD = 64
SPAN = 32


EPS_GROUP = 0.00064
EPS_NORM = 1e-06
HIGHEST = lax.Precision.HIGHEST


def prefix_2(shard, axis, join, neutral):
    place = lax.axis_index(axis)
    gathered = jax.tree.map(
        lambda a, kind: lax.all_gather(a.astype(kind), axis), shard, (jnp.bfloat16, jnp.bfloat16)
    )
    state = jax.tree.map(lambda a, e: jnp.zeros_like(a) + jnp.asarray(e, a.dtype), shard, neutral)

    def one(step, state):
        return join(
            state,
            jax.tree.map(
                lambda a, own: lax.dynamic_index_in_dim(a, step, 0, False).astype(own.dtype),
                gathered,
                shard,
            ),
        )

    return lax.fori_loop(0, place, one, state)


def exact_einsum(pattern, first_op, second_op):
    return jnp.einsum(pattern, first_op, second_op, precision=HIGHEST)


def block_pieces(recept, keyvec, valvec, logdec, unit_key, correction):
    span_len = recept.shape[1]
    cum_in = jnp.cumsum(logdec, axis=1)
    cum_ex = cum_in - logdec
    cum_end = cum_in[:, span_len - 1 :]
    growth = jnp.exp(-cum_in)
    r_scaled = recept * jnp.exp(cum_in)
    u_scaled = unit_key * jnp.exp(cum_ex)
    k_scaled = keyvec * growth
    c_scaled = correction * growth
    row_pos = lax.broadcasted_iota(jnp.int32, (span_len, span_len), 0)
    col_pos = lax.broadcasted_iota(jnp.int32, (span_len, span_len), 1)
    strict = (col_pos < row_pos).astype(jnp.float32)
    causal = (col_pos <= row_pos).astype(jnp.float32)
    key_pull = exact_einsum("bthn,bshn->bhts", u_scaled, k_scaled) * strict
    corr_pull = exact_einsum("bthn,bshn->bhts", u_scaled, c_scaled) * strict
    key_read = exact_einsum("bthn,bshn->bhts", r_scaled, k_scaled) * causal
    corr_read = exact_einsum("bthn,bshn->bhts", r_scaled, c_scaled) * causal
    system = corr_pull + jnp.eye(span_len, dtype=jnp.float32)
    right_local = exact_einsum("bhts,bshn->bhtn", key_pull, valvec)
    right_start = jnp.swapaxes(u_scaled, 1, 2)
    solved = jax.scipy.linalg.solve_triangular(
        system, jnp.concatenate([right_local, right_start], axis=-1), lower=True, unit_diagonal=True
    )
    channels = valvec.shape[-1]
    pulled_local = solved[..., :channels]
    reach_rows = solved[..., channels:]
    read_local = exact_einsum("bhts,bshn->bthn", key_read, valvec) - exact_einsum(
        "bhts,bhsn->bthn", corr_read, pulled_local
    )
    start_rows = r_scaled - exact_einsum("bhts,bhsn->bthn", corr_read, reach_rows)
    tail_decay = jnp.exp(cum_end - cum_in)
    c_tail = correction * tail_decay
    k_tail = keyvec * tail_decay
    keep_end = jnp.exp(cum_end[:, 0])
    block_map = keep_end[..., :, None] * jnp.eye(channels, dtype=jnp.float32) - exact_einsum(
        "bhtj,bthl->bhjl", reach_rows, c_tail
    )
    block_add = exact_einsum("bthi,bthl->bhil", valvec, k_tail) - exact_einsum(
        "bhti,bthl->bhil", pulled_local, c_tail
    )
    return (read_local, start_rows, block_map, block_add)


def time_mix(
    receptance, key_vectors, value_vectors, decay_logits, rate_logits, gate_logits, group_gain
):
    tokens_here, channels = receptance.shape
    heads_here = channels // HEAD
    block_shape = (tokens_here // SPAN, SPAN, heads_here, HEAD)

    def arrange(array):
        return array.astype(jnp.float32).reshape(block_shape)

    recept = arrange(receptance)
    keyvec = arrange(key_vectors)
    valvec = arrange(value_vectors)
    logdec = -jnp.exp(-jax.nn.softplus(-arrange(decay_logits)) - 0.5)
    unit_key = keyvec / jnp.sqrt(1.0 + jnp.sum(keyvec * keyvec, axis=-1, keepdims=True))
    correction = unit_key * jax.nn.sigmoid(arrange(rate_logits))
    read_local, start_rows, block_map, block_add = block_pieces(
        recept, keyvec, valvec, logdec, unit_key, correction
    )
    eye_heads = jnp.broadcast_to(jnp.eye(HEAD, dtype=jnp.float32), (heads_here, HEAD, HEAD))
    zero_heads = jnp.zeros((heads_here, HEAD, HEAD), jnp.float32)

    def advance(carried, inputs):
        local_state, product = carried
        step_map, step_add = inputs
        new_state = exact_einsum("hij,hjl->hil", local_state, step_map) + step_add
        new_product = exact_einsum("hij,hjl->hil", product, step_map)
        return ((new_state, new_product), (local_state, product))

    (device_add, device_map), (starts, products) = lax.scan(
        advance, (zero_heads, eye_heads), (block_map, block_add)
    )

    def compose(earlier, following):
        return (
            exact_einsum("hij,hjl->hil", earlier[0], following[0]),
            exact_einsum("hij,hjl->hil", earlier[1], following[0]) + following[1],
        )

    prefix = prefix_2((device_map, device_add), "sp", compose, (eye_heads, zero_heads))
    incoming = prefix[1]

    def replay(carried, inputs):
        rows_here, step_map, step_add = inputs
        following = exact_einsum("hij,hjl->hil", carried, step_map) + step_add
        return (following, exact_einsum("thj,hij->thi", rows_here, carried))

    final_state, from_start = lax.scan(replay, incoming, (start_rows, block_map, block_add))
    state_read = read_local + from_start
    centred = state_read - jnp.mean(state_read, axis=-1, keepdims=True)
    scaled = centred * lax.rsqrt(jnp.mean(centred * centred, axis=-1, keepdims=True) + EPS_GROUP)
    gated_out = (
        scaled.reshape(tokens_here, channels)
        * group_gain[None, :]
        * jax.nn.sigmoid(gate_logits.astype(jnp.float32))
    )
    return gated_out.astype(jnp.bfloat16)


def local(
    receptance,
    key_vectors,
    value_vectors,
    decay_logits,
    rate_logits,
    gate_logits,
    group_gain,
    residual,
    mixer_out,
    norm_gain,
    expert_ids,
    route_weight,
    expert_gate,
    expert_up,
    expert_down,
):
    mixed_rows = time_mix(
        receptance, key_vectors, value_vectors, decay_logits, rate_logits, gate_logits, group_gain
    )
    tokens_here, features = residual.shape
    projected = jnp.dot(
        lax.all_gather(mixed_rows, "tp", axis=1, tiled=True),
        mixer_out,
        preferred_element_type=jnp.float32,
    )
    midway = (residual.astype(jnp.float32) + projected).astype(jnp.bfloat16)
    midway_f = midway.astype(jnp.float32)
    squares = lax.psum(jnp.sum(midway_f * midway_f, axis=1), "tp")
    inv_rms = lax.rsqrt(squares / D + EPS_NORM)
    normed = (midway_f * norm_gain[None, :] * inv_rms[:, None]).astype(jnp.bfloat16)
    routes = expert_ids.shape[1]
    experts_all = lax.axis_size("sp") * expert_gate.shape[0]
    capacity = 2 * tokens_here * routes // experts_all
    flat_ids = expert_ids.reshape(-1)
    onehot = (flat_ids[:, None] == jnp.arange(experts_all, dtype=jnp.int32)[None, :]).astype(
        jnp.int32
    )
    earlier_count = jnp.sum((jnp.cumsum(onehot, axis=0) - onehot) * onehot, axis=1)
    slot_of = flat_ids * capacity + earlier_count
    owner_token = jnp.arange(tokens_here * routes, dtype=jnp.int32) // routes
    slot_table = (
        jnp.full((experts_all * capacity,), tokens_here, jnp.int32).at[slot_of].set(owner_token)
    )
    padded = jnp.concatenate([normed, jnp.zeros((1, features), jnp.bfloat16)], axis=0)
    outgoing = padded[slot_table].reshape(experts_all, capacity, features)
    arrived = lax.all_to_all(outgoing, "sp", split_axis=0, concat_axis=0, tiled=True)
    arrived_rows = arrived.reshape(-1, features)
    paired = jnp.concatenate([expert_gate[0], expert_up[0]], axis=1)
    gate_up = lax.psum_scatter(
        jnp.dot(arrived_rows, paired, preferred_element_type=jnp.float32).astype(jnp.bfloat16),
        "tp",
        scatter_dimension=0,
        tiled=True,
    ).astype(jnp.float32)
    half_width = paired.shape[1] // 2
    hidden = (jax.nn.silu(gate_up[:, :half_width]) * gate_up[:, half_width:]).astype(jnp.bfloat16)
    expert_res = jnp.dot(
        lax.all_gather(hidden, "tp", axis=0, tiled=True),
        expert_down[0],
        preferred_element_type=jnp.float32,
    )
    returned = lax.all_to_all(
        expert_res.astype(jnp.bfloat16).reshape(-1, capacity, features),
        "sp",
        split_axis=0,
        concat_axis=0,
        tiled=True,
    )
    picked = (
        returned.reshape(-1, features)[slot_of]
        .astype(jnp.float32)
        .reshape(tokens_here, routes, features)
    )
    routed_sum = jnp.sum(picked * route_weight[:, :, None], axis=1)
    return (midway_f + routed_sum).astype(jnp.bfloat16)


def solution(mesh):
    placed = (
        P("sp", "tp"),
        P("sp", "tp"),
        P("sp", "tp"),
        P("sp", "tp"),
        P("sp", "tp"),
        P("sp", "tp"),
        P("tp"),
        P("sp", "tp"),
        P(None, "tp"),
        P("tp"),
        P("sp", None),
        P("sp", None),
        P("sp", "tp", None),
        P("sp", "tp", None),
        P("sp", None, "tp"),
    )
    return jax.shard_map(
        local, mesh=mesh, in_specs=placed, out_specs=P("sp", "tp"), check_vma=False
    )
```

profile of v0, /device:TPU:9, one launch (start us, length us, event | category | flops | bytes accessed | tf_op | source)
XLA Modules:
  0.0 842.1 jit_solution(15395711707935724914)
XLA Ops:
  7.9 1.9 neg.31
  9.7 3.3 fusion.33
  15.7 2.7 reshape.171
  18.4 2.2 multiply_reduce_fusion.2
  20.8 2.3 add_divide_fusion
  23.1 2.8 div.42
  26.0 8.6 %fusion.61 = (f32[8,32,16,64]{3,1,2,0:T(8,128)S(1)}, f32[8,32,16,64]{3,1,2,0:T(8,128)}, f32[8,32,16,64]{3,1,2,0:T(8,128)S(1)}) fusion(f32[8,32,16,64]{3,2,1,0:T(8,128)} %copy-done.1, f32[8,32,16,64]{3,2,1,0:T(8,128)} %div.42, f32[8,32,16]{1,2,0:T(8,128)S(1)} %add_sqrt_fusion, f32[8,32,16,64]{3,2,1,0:T(8,128)} %reshape.171, ...), kind=kLoop, calls=%fused_computation.81 | loop fusion | flops 4456448 | bytes 7389184 | tf_op jit(solution)/shard_map/mul | solution.py:49
  34.6 6.0 fusion.86
  40.6 4.9 add_bitcast_fusion
  45.4 316.9 %custom-call.4 = f32[8,16,1,32,32]{3,4,2,1,0:T(8,128)} custom-call(f32[8,16,1,32,32]{4,3,2,1,0:T(8,128)} %add_bitcast_fusion), custom_call_target="InvertDiagBlocksLowerTriangular" | custom-call | tf_op jit(solution)/shard_map/jit(_solve_triangular)/vmap(vmap())/triangular_solve | solution.py:61
  362.3 2.7 reshape.160
  365.0 3.4 fusion.45
  368.4 4.0 fusion.34
  373.8 7.3 fusion.52
  381.2 5.7 bitcast_subtract_fusion
  387.0 12.5 %multiply_subtract_fusion = f32[8,16,64,64]{3,2,1,0:T(8,128)} fusion(f32[8,32,16,64]{3,1,2,0:T(8,128)} %get-tuple-element.218, f32[64,64]{1,0:T(8,128)S(1)} %fusion.90, f32[8,16,64]{2,1,0:T(8,128)S(1)} %fusion.106, f32[8,16,32,128]{3,2,1,0:T(8,128)} %copy-done.8), kind=kOutput, calls=%fused_computation.38 | convolution fusion | flops 202375168 | bytes 5292032 | tf_op jit(solution)/shard_map/bhtj,bthl->bhjl/dot_general | solution.py:37
  399.5 5.4 copy.131
  405.0 29.5 %while.42 = (s32[]{:T(128)}, f32[16,64,64]{1,2,0:T(8,128)S(1)}, f32[16,64,64]{1,2,0:T(8,128)S(1)}, f32[8,16,64,64]{2,3,1,0:T(8,128)}, f32[8,16,64,64]{2,3,1,0:T(8,128)}) while((s32[]{:T(128)}, f32[16,64,64]{1,2,0:T(8,128)S(1)}, f32[16,64,64]{1,2,0:T(8,128)S(1)}, f32[8,16,64,64]{2,3,1,0:T(8,128)}, ...), condition=%wide.region_3.4_spmd.clone.clone, body=%wide.region_2.3_spmd.clone.sunk.clone | while | flops 100794368 | bytes 3671623 | solution.py:113
  405.0 1.9 fusion.164
  408.7 1.9 fusion.164
  412.4 1.9 fusion.164
  416.1 1.9 fusion.164
  419.8 1.9 fusion.164
  423.5 1.9 fusion.164
  427.1 1.9 fusion.164
  430.8 1.9 fusion.164
  436.3 3.0 reshape.169
  439.3 7.7 fusion.107
  447.0 3.6 fusion.54
  450.6 6.7 fusion.88
  457.3 4.7 bitcast_subtract_fusion.1
  462.0 4.1 all-gather.11.cloned.1.call-done
  466.2 30.2 %all-gather.13.cloned.1.call-done = bf16[128,64,64]{2,1,0:T(8,128)(2,1)} async-done(((bf16[16,64,64]{2,1,0:T(8,128)(2,1)}), bf16[128,64,64]{2,1,0:T(8,128)(2,1)}) %all-gather.13.cloned.1.call-update) | async-done | bytes 1048592 | tf_op jit(solution)/shard_map/all_gather | solution.py:19
  496.4 7.9 while.40
  504.3 33.3 %while.41 = (s32[]{:T(128)}, f32[16,64,64]{1,2,0:T(8,128)S(1)}, f32[8,32,16,64]{3,1,2,0:T(8,128)}, f32[8,16,64,64]{2,3,1,0:T(8,128)}, f32[8,16,64,64]{2,3,1,0:T(8,128)}, /*index=5*/f32[8,32,16,64]{3,1,2,0:T(8,128)}) while((s32[]{:T(128)}, f32[16,64,64]{1,2,0:T(8,128)S(1)}, f32[8,32,16,64]{3,1,2,0:T(8,128)}, ...), condition=%wide.region_7.8_spmd.clone, body=%wide.region_6.7_spmd.sunk.clone | while | flops 75563008 | bytes 2885701 | solution.py:131
  504.4 2.3 fusion.159
  506.7 1.8 fusion.158
  508.6 2.3 fusion.159
  510.8 1.8 fusion.158
  512.7 2.2 fusion.159
  516.9 2.3 fusion.159
  521.0 2.3 fusion.159
  525.2 2.3 fusion.159
  529.4 2.2 fusion.159
  533.5 2.2 fusion.159
  537.6 5.1 fusion.108
  545.3 2.5 copy.137
  547.8 2.0 reshape.161
  549.8 2.1 multiply_convert_fusion
  554.7 2.4 scatter_custom_fusion
  557.2 39.4 %all-gather.7.cloned.1.call-done = bf16[256,4096]{1,0:T(8,128)(2,1)} async-done(((bf16[256,1024]{1,0:T(8,128)(2,1)}), bf16[256,4096]{1,0:T(8,128)(2,1)}) %all-gather.7.cloned.1.call-update) | async-done | bytes 2097168 | tf_op jit(solution)/shard_map/all_gather | solution.py:165
  596.6 6.5 fusion.75
  603.1 6.9 psum.7
  610.2 5.4 gather_fusion
  615.6 53.9 %all_to_all.10 = bf16[8,128,1024]{2,1,0:T(8,128)(2,1)S(1)} all-to-all(bf16[8,128,1024]{2,1,0:T(8,128)(2,1)} %bitcast.153), channel_id=1, replica_groups=mesh['sp'=8,'tp'=4] {'sp'}, dimensions={0} | all-to-all | bytes 4194304 | tf_op jit(solution)/shard_map/all_to_all | solution.py:189
  669.5 6.2 fusion.27
  675.9 52.7 %reduce-scatter.2.cloned.1.call-done = bf16[256,2048]{1,0:T(8,128)(2,1)} async-done(((bf16[1024,2048]{1,0:T(8,128)(2,1)}), bf16[256,2048]{1,0:T(8,128)(2,1)}) %reduce-scatter.2.cloned.1.call-update) | async-done | bytes 1048592 | tf_op jit(solution)/shard_map/reduce_scatter | solution.py:192
  731.1 35.3 %all-gather.9.cloned.1.call-done = bf16[1024,1024]{1,0:T(8,128)(2,1)} async-done(((bf16[256,1024]{1,0:T(8,128)(2,1)}), bf16[1024,1024]{1,0:T(8,128)(2,1)}) %all-gather.9.cloned.1.call-update) | async-done | bytes 2097168 | tf_op jit(solution)/shard_map/all_gather | solution.py:201
  766.5 5.3 fusion.58
  771.7 5.9 all-to-all-start.1
  777.9 45.3 %all-to-all-done.1 = bf16[8,128,1024]{2,1,0:T(8,128)(2,1)} async-done(((bf16[8,128,1024]{2,1,0:T(8,128)(2,1)}), bf16[8,128,1024]{2,1,0:T(8,128)(2,1)}, u32[]{:S(2)}, u32[]{:S(2)}) %all-to-all-start.1) | async-done | bytes 2097184 | tf_op jit(solution)/shard_map/all_to_all | solution.py:205
  823.2 4.6 gather_fusion.1
  827.8 2.3 reshape.172
  830.1 4.3 multiply_reduce_fusion
  (155 shorter events, 50.2 us)
Async XLA Ops:
  6.5 759.9 %copy-start = (bf16[1,1024,1024]{2,1,0:T(8,128)(2,1)S(1)}, bf16[1,1024,1024]{2,1,0:T(8,128)(2,1)}, u32[]{:S(2)}) copy-start(bf16[1,1024,1024]{2,1,0:T(8,128)(2,1)} %param.35) | copy-start | bytes 6291460
  6.5 459.6 %all-gather.11.cloned.1.call-start = ((), (), s32[]{:S(2)}) async-start(), calls=%async_computation.6 | async-start | bytes 2359296 | tf_op jit(solution)/shard_map/all_gather | solution.py:19
  14.4 1.3 copy-start.1
  26.0 8.6 %copy-start.2 = (f32[8,32,16,64]{3,2,1,0:T(8,128)S(1)}, f32[8,32,16,64]{3,2,1,0:T(8,128)}, u32[]{:S(2)}) copy-start(f32[8,32,16,64]{3,2,1,0:T(8,128)} %copy-done.1) | copy-start | bytes 3145732
  26.0 8.6 %copy-start.5 = (f32[8,32,16,64]{3,2,1,0:T(8,128)S(1)}, f32[8,32,16,64]{3,2,1,0:T(8,128)}, u32[]{:S(2)}) copy-start(f32[8,32,16,64]{3,2,1,0:T(8,128)} %reshape.171) | copy-start | bytes 3145732
  34.5 6.0 copy-start.11
  34.5 6.0 copy-start.13
  365.0 3.4 copy-start.12
  365.0 3.4 copy-start.18
  368.4 5.4 copy-start.14
  372.5 1.4 copy-start.8
  373.8 7.4 copy-start.3
  373.8 7.4 copy-start.6
  373.8 7.4 copy-start.15
  435.3 61.0 %all-gather.13.cloned.1.call-start = ((), (), s32[]{:S(2)}) async-start(), calls=%async_computation.7 | async-start | bytes 2359296 | tf_op jit(solution)/shard_map/all_gather | solution.py:19
  436.2 160.4 %all-gather.7.cloned.1.call-start = ((), (), s32[]{:S(2)}) async-start(), calls=%async_computation.3 | async-start | bytes 2621440 | tf_op jit(solution)/shard_map/all_gather | solution.py:165
  439.3 7.7 copy-start.9
  447.0 3.6 copy-start.4
  447.0 3.6 copy-start.7
  447.0 3.6 copy-start.10
  547.8 2.0 copy-start.20
  549.8 2.2 copy-start.19
  552.0 176.5 %reduce-scatter.2.cloned.1.call-start = ((), (), s32[]{:S(2)}) async-start(), calls=%async_computation.4 | async-start | bytes 5242880 | tf_op jit(solution)/shard_map/reduce_scatter | solution.py:192
  557.2 52.8 %copy-start.21 = (f32[1024]{0:T(1024)S(1)}, f32[1024]{0:T(1024)}, u32[]{:S(2)}) copy-start(f32[1024]{0:T(1024)} %param.30) | copy-start | bytes 12292
  603.1 6.9 copy-start.16
  615.6 53.9 %copy-start.23 = (bf16[1,1024,1024]{2,1,0:T(8,128)(2,1)S(1)}, bf16[1,1024,1024]{2,1,0:T(8,128)(2,1)}, u32[]{:S(2)}) copy-start(bf16[1,1024,1024]{2,1,0:T(8,128)(2,1)} %param.34) | copy-start | bytes 6291460
  615.6 53.9 %copy-start.24 = (bf16[1,1024,1024]{2,1,0:T(8,128)(2,1)S(1)}, bf16[1,1024,1024]{2,1,0:T(8,128)(2,1)}, u32[]{:S(2)}) copy-start(bf16[1,1024,1024]{2,1,0:T(8,128)(2,1)} %param.33) | copy-start | bytes 6291460
  675.8 90.6 %all-gather.9.cloned.1.call-start = ((), (), s32[]{:S(2)}) async-start(), calls=%async_computation.5 | async-start | bytes 2621440 | tf_op jit(solution)/shard_map/all_gather | solution.py:201
  771.7 6.0 copy-start.22
  771.7 51.4 %all-to-all-start.1 = ((bf16[8,128,1024]{2,1,0:T(8,128)(2,1)}), bf16[8,128,1024]{2,1,0:T(8,128)(2,1)}, u32[]{:S(2)}, u32[]{:S(2)}) async-start(bf16[8,128,1024]{2,1,0:T(8,128)(2,1)} %bitcast.154), calls=%async_computation.2 | async-start | bytes 4194304 | tf_op jit(solution)/shard_map/all_to_all | solution.py:205
  830.1 4.3 copy-start.17
Sparse Core Ops, SparseCore 0:
  435.5 30.6 all-gather.10
  467.8 28.5 all-gather.12
  552.1 44.4 all-gather.6
  675.9 52.5 reduce-scatter.1
  731.2 35.1 all-gather.8
where the time goes:
time: 855 us; the launch traced here: 842 us
  other arithmetic  350 us (41%)
  waiting for transfers between devices  207 us (24%)
  matrix products  155 us (18%)
  blocking collectives  60.8 us (7%)
  local copies, waits for them, and re-layouts  48 us (6%)
  between operations  13.9 us (2%)
    another operation x3, other arithmetic, block_pieces(): jax.scipy.linalg.solve_triangular(system, jnp.concatenate([right_local, r...  317 us
    dot_general x46, matrix products, exact_einsum(): return jnp.einsum(pattern, first_op, second_op, precision=HIGHEST)  133 us
    all_to_all x1, blocking collectives, local(): lax.all_to_all(outgoing, 'sp', split_axis=0, concat_axis=0, tiled=True)  53.9 us
    reduce_scatter x1, waiting for transfers between devices, local(): lax.psum_scatter(jnp.dot(arrived_rows, paired, preferred_element_type=jnp...  52.7 us
    all_to_all x1, waiting for transfers between devices, local(): lax.all_to_all(expert_res.astype(jnp.bfloat16).reshape(-1, capacity, feat...  45.3 us
    all_gather x1, waiting for transfers between devices, local(): lax.all_gather(mixed_rows, 'tp', axis=1, tiled=True)  39.4 us
    all_gather x1, waiting for transfers between devices, local(): lax.all_gather(hidden, 'tp', axis=0, tiled=True)  35.3 us
    all_gather x2, waiting for transfers between devices, prefix_2(): lax.all_gather(a.astype(kind), axis)  34.3 us
  transfers between devices with their start and end apart: 6, of which 6 were waited for; matrix products, arithmetic and copies ran while one was open for 4% of the time, Pallas kernels for 0%

commit v1 on v0

v1 whole, which is shorter than its diff:
```python
import jax
import jax.numpy as jnp
from jax import lax
from jax.experimental import pallas as pl
from jax.experimental.pallas import tpu as pltpu
from jax.sharding import PartitionSpec as P

D = 4096
HEAD = 64
CHUNK = 128
EXP_HALF = 0.6065306597126334


EPS_GROUP = 0.00064
EPS_NORM = 1e-06


def split(x):
    hi = x.astype(jnp.bfloat16)
    lo = (x - hi.astype(jnp.float32)).astype(jnp.bfloat16)
    return hi, lo


def dot(a, b, dims):
    return lax.dot_general(a, b, (dims, ((), ())), preferred_element_type=jnp.float32)


NN = ((1,), (0,))
NT = ((1,), (1,))
TN = ((0,), (0,))


def dot3(a, b, dims=NN):
    return dot(a[0], b[0], dims) + (dot(a[0], b[1], dims) + dot(a[1], b[0], dims))


def dot2(a, b, dims=NN):
    return dot(a[0], b, dims) + dot(a[1], b, dims)


def sigmoid(x):
    return 1.0 / (1.0 + jnp.exp(-x))


def mix_kernel(r_ref, k_ref, v_ref, d_ref, a_ref, out_ref, state_ref):
    tokens = r_ref.shape[0]
    chunks = tokens // CHUNK
    row = lax.broadcasted_iota(jnp.int32, (CHUNK, CHUNK), 0)
    col = lax.broadcasted_iota(jnp.int32, (CHUNK, CHUNK), 1)
    strict = col < row
    causal = col <= row
    eye = jnp.where(col == row, 1.0, 0.0)
    ones_lower = jnp.where(causal, 1.0, 0.0).astype(jnp.bfloat16)
    low = lax.broadcasted_iota(jnp.int32, (CHUNK, 2 * HEAD), 1) < HEAD

    work = []
    for chunk in range(chunks):
        rows = pl.ds(chunk * CHUNK, CHUNK)
        recept = r_ref[rows, :].astype(jnp.float32)
        keyvec = k_ref[rows, :].astype(jnp.float32)
        logdec = -EXP_HALF * sigmoid(d_ref[rows, :].astype(jnp.float32))
        first, second = split(logdec)
        third = (logdec - first.astype(jnp.float32) - second.astype(jnp.float32)).astype(jnp.bfloat16)
        cum_in = dot(ones_lower, first, NN) + (
            dot(ones_lower, second, NN) + dot(ones_lower, third, NN)
        )
        cum_end = cum_in[CHUNK - 1 :, :]
        squares = keyvec * keyvec
        norms = jnp.where(
            low,
            jnp.sum(squares[:, :HEAD], axis=1, keepdims=True),
            jnp.sum(squares[:, HEAD:], axis=1, keepdims=True),
        )
        unit_key = keyvec * lax.rsqrt(1.0 + norms)
        correction = unit_key * sigmoid(a_ref[rows, :].astype(jnp.float32))
        growth = jnp.exp(-cum_in)
        tail = jnp.exp(cum_end - cum_in)
        r_scaled = recept * jnp.exp(cum_in)
        u_scaled = unit_key * jnp.exp(cum_in - logdec)
        queries = split(jnp.concatenate([u_scaled, r_scaled], axis=0))
        sources = split(jnp.concatenate([keyvec * growth, correction * growth], axis=0))
        tails = split(jnp.concatenate([keyvec * tail, -(correction * tail)], axis=0))
        keep = jnp.broadcast_to(jnp.exp(cum_end), (2 * HEAD, 2 * HEAD)).T
        values = v_ref[rows, :]
        for head in range(2):
            lanes = slice(head * HEAD, (head + 1) * HEAD)
            query = tuple(q[:, lanes] for q in queries)
            source = tuple(s[:, lanes] for s in sources)
            scores = dot3(query, source, NT)
            work.append(
                dict(
                    head=head,
                    chunk=chunk,
                    query=query,
                    tail=tuple(t[:, lanes] for t in tails),
                    keep=keep[lanes, :],
                    value=jnp.concatenate(
                        [values[:, lanes], jnp.zeros((CHUNK, HEAD), jnp.bfloat16)], axis=1
                    ),
                    key_both=split(
                        jnp.concatenate(
                            [
                                jnp.where(strict, scores[:CHUNK, :CHUNK], 0.0),
                                jnp.where(causal, scores[CHUNK:, :CHUNK], 0.0),
                            ],
                            axis=0,
                        )
                    ),
                    pull=jnp.where(strict, scores[:CHUNK, CHUNK:], 0.0),
                    corr_read=split(jnp.where(causal, scores[CHUNK:, CHUNK:], 0.0)),
                )
            )
    for item in work:
        item["inverse"] = eye - jnp.where(row // 2 == col // 2, item["pull"], 0.0)
        item["from_values"] = dot2(item["key_both"], item["value"])
    size = 2
    while size < CHUNK:
        joined = (row // (2 * size) == col // (2 * size)) & (row // size != col // size)
        halves = []
        for item in work:
            inverse = split(item["inverse"])
            between = split(jnp.where(joined, item["pull"], 0.0))
            halves.append((inverse, dot3(between, inverse)))
        for item, (inverse, half) in zip(work, halves):
            item["inverse"] = item["inverse"] - dot3(inverse, split(half))
        size *= 2
    key_row = lax.broadcasted_iota(jnp.int32, (HEAD, 2 * HEAD), 0)
    lane = lax.broadcasted_iota(jnp.int32, (HEAD, 2 * HEAD), 1)
    start = jnp.where(lane == key_row + HEAD, 1.0, 0.0)
    states = [start, start]
    for item in work:
        head = item["head"]
        state = states[head]
        from_start = dot3(item["query"], split(state)) + item["from_values"]
        pulled = dot3(split(item["inverse"]), split(from_start[:CHUNK]))
        pulled_parts = split(pulled)
        out_ref[pl.ds(item["chunk"] * CHUNK, CHUNK), pl.ds(head * 2 * HEAD, 2 * HEAD)] = (
            from_start[CHUNK:] - dot3(item["corr_read"], pulled_parts)
        )
        key_tail = tuple(t[:CHUNK] for t in item["tail"])
        corr_tail = tuple(t[CHUNK:] for t in item["tail"])
        states[head] = (
            item["keep"] * state
            + dot2(key_tail, item["value"], TN)
            + dot3(corr_tail, pulled_parts, TN)
        )
    for head in range(2):
        state_ref[pl.ds(head * HEAD, HEAD), :] = states[head].astype(jnp.bfloat16)


def read_kernel(place_ref, read_ref, maps_ref, gate_ref, gain_ref, out_ref):
    def one(step, carried):
        following = []
        for head in range(2):
            both = maps_ref[step, pl.ds(head * HEAD, HEAD), :]
            parts = split(carried[head])
            step_map = both[:, HEAD:]
            following.append(
                both[:, :HEAD].astype(jnp.float32)
                + dot(step_map, parts[0], NN)
                + dot(step_map, parts[1], NN)
            )
        return tuple(following)

    zero = jnp.zeros((HEAD, HEAD), jnp.float32)
    incoming = lax.fori_loop(0, place_ref[0], one, (zero, zero))
    scaled = []
    for head in range(2):
        both = read_ref[:, pl.ds(head * 2 * HEAD, 2 * HEAD)]
        state_read = both[:, :HEAD] + dot3(split(both[:, HEAD:]), split(incoming[head]))
        centred = state_read - jnp.mean(state_read, axis=1, keepdims=True)
        variance = jnp.mean(centred * centred, axis=1, keepdims=True)
        scaled.append(centred * lax.rsqrt(variance + EPS_GROUP))
    gated = (
        jnp.concatenate(scaled, axis=1)
        * gain_ref[...]
        * sigmoid(gate_ref[...].astype(jnp.float32))
    )
    out_ref[...] = gated.astype(jnp.bfloat16)


def time_mix(
    receptance, key_vectors, value_vectors, decay_logits, rate_logits, gate_logits, group_gain
):
    tokens_here, channels = receptance.shape
    pairs = channels // (2 * HEAD)
    wide = pl.BlockSpec((tokens_here, 2 * HEAD), lambda i: (0, i))
    double = pl.BlockSpec((tokens_here, 4 * HEAD), lambda i: (0, i))
    reads, states = pl.pallas_call(
        mix_kernel,
        grid=(pairs,),
        in_specs=[wide] * 5,
        out_specs=[double, pl.BlockSpec((2 * HEAD, 2 * HEAD), lambda i: (i, 0))],
        out_shape=[
            jax.ShapeDtypeStruct((tokens_here, 2 * channels), jnp.float32),
            jax.ShapeDtypeStruct((channels, 2 * HEAD), jnp.bfloat16),
        ],
        name="mix",
    )(receptance, key_vectors, value_vectors, decay_logits, rate_logits)
    maps = lax.all_gather(states, "sp")
    place = lax.axis_index("sp").astype(jnp.int32).reshape(1)
    return pl.pallas_call(
        read_kernel,
        grid=(pairs,),
        in_specs=[
            pl.BlockSpec(memory_space=pltpu.SMEM),
            double,
            pl.BlockSpec((maps.shape[0], 2 * HEAD, 2 * HEAD), lambda i: (0, i, 0)),
            wide,
            pl.BlockSpec((1, 2 * HEAD), lambda i: (0, i)),
        ],
        out_specs=wide,
        out_shape=jax.ShapeDtypeStruct((tokens_here, channels), jnp.bfloat16),
        name="read",
    )(place, reads, maps, gate_logits, group_gain.reshape(1, channels))


def local(
    receptance,
    key_vectors,
    value_vectors,
    decay_logits,
    rate_logits,
    gate_logits,
    group_gain,
    residual,
    mixer_out,
    norm_gain,
    expert_ids,
    route_weight,
    expert_gate,
    expert_up,
    expert_down,
):
    mixed_rows = time_mix(
        receptance, key_vectors, value_vectors, decay_logits, rate_logits, gate_logits, group_gain
    )
    tokens_here, features = residual.shape
    projected = jnp.dot(
        lax.all_gather(mixed_rows, "tp", axis=1, tiled=True),
        mixer_out,
        preferred_element_type=jnp.float32,
    )
    midway = (residual.astype(jnp.float32) + projected).astype(jnp.bfloat16)
    midway_f = midway.astype(jnp.float32)
    squares = lax.psum(jnp.sum(midway_f * midway_f, axis=1), "tp")
    inv_rms = lax.rsqrt(squares / D + EPS_NORM)
    normed = (midway_f * norm_gain[None, :] * inv_rms[:, None]).astype(jnp.bfloat16)
    routes = expert_ids.shape[1]
    experts_all = lax.axis_size("sp") * expert_gate.shape[0]
    capacity = 2 * tokens_here * routes // experts_all
    flat_ids = expert_ids.reshape(-1)
    onehot = (flat_ids[:, None] == jnp.arange(experts_all, dtype=jnp.int32)[None, :]).astype(
        jnp.int32
    )
    earlier_count = jnp.sum((jnp.cumsum(onehot, axis=0) - onehot) * onehot, axis=1)
    slot_of = flat_ids * capacity + earlier_count
    owner_token = jnp.arange(tokens_here * routes, dtype=jnp.int32) // routes
    slot_table = (
        jnp.full((experts_all * capacity,), tokens_here, jnp.int32).at[slot_of].set(owner_token)
    )
    padded = jnp.concatenate([normed, jnp.zeros((1, features), jnp.bfloat16)], axis=0)
    outgoing = padded[slot_table].reshape(experts_all, capacity, features)
    arrived = lax.all_to_all(outgoing, "sp", split_axis=0, concat_axis=0, tiled=True)
    arrived_rows = arrived.reshape(-1, features)
    paired = jnp.concatenate([expert_gate[0], expert_up[0]], axis=1)
    gate_up = lax.psum_scatter(
        jnp.dot(arrived_rows, paired, preferred_element_type=jnp.float32).astype(jnp.bfloat16),
        "tp",
        scatter_dimension=0,
        tiled=True,
    ).astype(jnp.float32)
    half_width = paired.shape[1] // 2
    hidden = (jax.nn.silu(gate_up[:, :half_width]) * gate_up[:, half_width:]).astype(jnp.bfloat16)
    expert_res = jnp.dot(
        lax.all_gather(hidden, "tp", axis=0, tiled=True),
        expert_down[0],
        preferred_element_type=jnp.float32,
    )
    returned = lax.all_to_all(
        expert_res.astype(jnp.bfloat16).reshape(-1, capacity, features),
        "sp",
        split_axis=0,
        concat_axis=0,
        tiled=True,
    )
    picked = (
        returned.reshape(-1, features)[slot_of]
        .astype(jnp.float32)
        .reshape(tokens_here, routes, features)
    )
    routed_sum = jnp.sum(picked * route_weight[:, :, None], axis=1)
    return (midway_f + routed_sum).astype(jnp.bfloat16)


def solution(mesh):
    placed = (
        P("sp", "tp"),
        P("sp", "tp"),
        P("sp", "tp"),
        P("sp", "tp"),
        P("sp", "tp"),
        P("sp", "tp"),
        P("tp"),
        P("sp", "tp"),
        P(None, "tp"),
        P("tp"),
        P("sp", None),
        P("sp", None),
        P("sp", "tp", None),
        P("sp", "tp", None),
        P("sp", None, "tp"),
    )
    return jax.shard_map(
        local, mesh=mesh, in_specs=placed, out_specs=P("sp", "tp"), check_vma=False
    )
```

time: 855 us -> 383 us (0.45)
  other arithmetic: 350 us -> 9.32 us
  matrix products: 155 us -> 17.9 us
  Pallas kernels: 0 us -> 54.6 us
  local copies, waits for them, and re-layouts: 48 us -> 15.9 us
    another operation x6 -> x2, other arithmetic: 320 us -> 1.18 us  [the longest x3 317 us: block_pieces(): jax.scipy.linalg.solve_triangular(system, jnp.concatenate([right_local, r...]
    dot_general x46 -> x0, matrix products: 133 us -> none  [exact_einsum(): return jnp.einsum(pattern, first_op, second_op, precision=HIGHEST)]
    pallas_call x0 -> x2, Pallas kernels: none -> 54.6 us  [the longest x1 42.8 us: time_mix(): pl.pallas_call(mix_kernel, grid=(pairs,), in_specs=[wide] * 5, out_specs=...]
    reshape x4 -> x0, local copies, waits for them, and re-layouts: 10.4 us -> none  [the longest x3 8.37 us: arrange(): return array.astype(jnp.float32).reshape(block_shape)]
    mul x2 -> x0, other arithmetic: 9.8 us -> none  [the longest x1 8.55 us: block_pieces(): c_scaled = correction * growth]
    all_gather x2 -> x1, waiting for transfers between devices: 34.3 us -> 30.8 us  [time_mix(): maps = lax.all_gather(states, 'sp')]
  transfers between devices with their start and end apart: 6 -> 5, of which waited for: 6 -> 5; matrix products, arithmetic and copies ran while one was open for 4% -> 1% of each run, Pallas kernels for 0% -> 0%
where the time goes in v1:
time: 383 us; the launch traced here: 378 us
  waiting for transfers between devices  200 us (52%)
  blocking collectives  60.8 us (16%)
  Pallas kernels  54.6 us (14%)
  matrix products  17.9 us (5%)
  local copies, waits for them, and re-layouts  15.9 us (4%)
  between operations  13.3 us (3%)
  other arithmetic  9.32 us (2%)
  starting transfers between devices  6.03 us (2%)
    all_to_all x1, blocking collectives, local(): lax.all_to_all(outgoing, 'sp', split_axis=0, concat_axis=0, tiled=True)  53.9 us
    reduce_scatter x1, waiting for transfers between devices, local(): lax.psum_scatter(jnp.dot(arrived_rows, paired, preferred_element_type=jnp...  52.5 us
    all_to_all x1, waiting for transfers between devices, local(): lax.all_to_all(expert_res.astype(jnp.bfloat16).reshape(-1, capacity, feat...  45.4 us
    pallas_call x1, Pallas kernels, time_mix(): pl.pallas_call(mix_kernel, grid=(pairs,), in_specs=[wide] * 5, out_specs=...  42.8 us
    all_gather x1, waiting for transfers between devices, local(): lax.all_gather(mixed_rows, 'tp', axis=1, tiled=True)  36 us
    all_gather x1, waiting for transfers between devices, local(): lax.all_gather(hidden, 'tp', axis=0, tiled=True)  35.3 us
    all_gather x1, waiting for transfers between devices, time_mix(): maps = lax.all_gather(states, 'sp')  30.8 us
    pallas_call x1, Pallas kernels, time_mix(): pl.pallas_call(read_kernel, grid=(pairs,), in_specs=[pl.BlockSpec(memory_...  11.8 us
  transfers between devices with their start and end apart: 5, of which 5 were waited for; matrix products, arithmetic and copies ran while one was open for 1% of the time, Pallas kernels for 0%

profile of v1, /device:TPU:9, one launch (start us, length us, event | category | flops | bytes accessed | tf_op | source)
XLA Modules:
  0.0 378.0 jit_solution(14063956986548874782)
XLA Ops:
  6.5 0.0 copy-start
  6.5 0.0 all-gather.9.cloned.1.call-start
  6.5 42.8 %mix.1 = (f32[256,2048]{1,0:T(8,128)}, bf16[1024,128]{1,0:T(8,128)(2,1)}) custom-call(bf16[256,1024]{1,0:T(8,128)(2,1)} %r_ref.1, bf16[256,1024]{1,0:T(8,128)(2,1)} %k_ref.1, bf16[256,1024]{1,0:T(8,128)(2,1)} %v_ref.1, bf16[256,1024]{1,0:T(8,128)(2,1)} %d_ref.1, bf16[256,1024]{1,0:T(8,128)(2,1)} %a_ref.1), custom_call_target="tpu_custom_call" | custom-call | tf_op jit(solution)/shard_map/mix/pallas_call | solution.py:189
  49.3 0.0 all-gather.9.cloned.1.call-update
  49.3 0.0 all-gather.5.cloned.1.call-start
  49.4 30.8 %all-gather.9.cloned.1.call-done = bf16[8192,128]{1,0:T(8,128)(2,1)} async-done(((bf16[1024,128]{1,0:T(8,128)(2,1)}), bf16[8192,128]{1,0:T(8,128)(2,1)}) %all-gather.9.cloned.1.call-update) | async-done | bytes 2097168 | tf_op jit(solution)/shard_map/all_gather | solution.py:200
  80.2 0.0 copy-start.3
  80.2 0.0 copy-start.8
  80.2 11.8 %read.1 = bf16[256,1024]{1,0:T(8,128)(2,1)} custom-call(s32[1]{0:T(128)} %bitcast.place_ref, f32[256,2048]{1,0:T(8,128)} %get-tuple-element.7.read_ref, bf16[8,1024,128]{2,1,0:T(8,128)(2,1)} %bitcast.29, bf16[256,1024]{1,0:T(8,128)(2,1)} %gate_ref.1, f32[1,1024]{1,0:T(1,128)} %bitcast.35), custom_call_target="tpu_custom_call" | custom-call | tf_op jit(solution)/shard_map/read/pallas_call | solution.py:202
  92.0 0.0 all-gather.5.cloned.1.call-update
  92.0 0.0 reduce-scatter.2.cloned.1.call-start
  92.1 0.0 copy-done.3
  92.1 0.1 copy.18
  92.2 0.1 eq.29
  92.4 0.1 eq.25
  92.5 1.1 reduce-window.6
  93.7 0.2 slice_reduce_fusion
  93.9 0.1 copy.17
  94.1 0.1 mul.60
  94.2 0.1 fusion.19
  94.3 2.4 scatter_custom_fusion
  96.8 0.0 copy-start.4
  96.8 36.0 %all-gather.5.cloned.1.call-done = bf16[256,4096]{1,0:T(8,128)(2,1)} async-done(((bf16[256,1024]{1,0:T(8,128)(2,1)}), bf16[256,4096]{1,0:T(8,128)(2,1)}) %all-gather.5.cloned.1.call-update) | async-done | bytes 2097168 | tf_op jit(solution)/shard_map/all_gather | solution.py:240
  132.9 0.0 copy-done.8
  132.9 6.5 %fusion.15 = (f32[256]{0:T(256)S(1)}, bf16[256,1024]{1,0:T(8,128)(2,1)S(1)}) fusion(bf16[256,4096]{1,0:T(8,128)(2,1)} %all-gather.5.cloned.1.call-done, bf16[4096,1024]{1,0:T(8,128)(2,1)} %param.23, bf16[256,1024]{1,0:T(8,128)(2,1)S(1)} %copy-done.8), kind=kOutput, calls=%fused_computation.19 | convolution fusion | flops 2149056256 | bytes 11535360 | tf_op jit(solution)/shard_map/dot_general | solution.py:239
  139.3 0.0 copy-start.1
  139.3 6.9 %psum.7 = f32[256]{0:T(256)S(1)} all-reduce(f32[256]{0:T(256)S(1)} %get-tuple-element.9), channel_id=1, replica_groups=mesh['sp'=8,'tp'=4] {'tp'}, use_global_device_ids=true, to_apply=%region_1.0 | all-reduce | flops 256 | bytes 2048 | tf_op jit(solution)/shard_map/psum | solution.py:246
  146.3 0.0 copy-done.1
  146.3 0.0 copy-done.4
  146.3 0.2 fusion.14
  146.5 5.4 %gather_fusion = bf16[1024,1024]{1,0:T(8,128)(2,1)} fusion(bf16[257,1024]{1,0:T(8,128)(2,1)S(1)} %concatenate.6, s32[1024]{0:T(1024)S(1)} %fusion.21), kind=kCustom, calls=%fused_computation | custom fusion | bytes 4198400 | tf_op jit(solution)/shard_map/gather | solution.py:263
  151.9 0.0 copy-start.6
  151.9 0.0 copy-start.7
  151.9 53.9 %all_to_all.10 = bf16[8,128,1024]{2,1,0:T(8,128)(2,1)S(1)} all-to-all(bf16[8,128,1024]{2,1,0:T(8,128)(2,1)} %bitcast.28), channel_id=1, replica_groups=mesh['sp'=8,'tp'=4] {'sp'}, dimensions={0} | all-to-all | bytes 4194304 | tf_op jit(solution)/shard_map/all_to_all | solution.py:264
  205.8 0.0 copy-done.6
  205.8 0.0 copy-done.7
  205.8 6.2 %fusion.4 = bf16[1024,2048]{1,0:T(8,128)(2,1)} fusion(bf16[1024,1024]{1,0:T(8,128)(2,1)S(1)} %bitcast.31, bf16[1024,1024]{1,0:T(8,128)(2,1)S(1)} %bitcast.36, bf16[1024,1024]{1,0:T(8,128)(2,1)S(1)} %bitcast.37), kind=kOutput, calls=%fused_computation.7 | convolution fusion | flops 4305453056 | bytes 10485760 | tf_op jit(solution)/shard_map/dot_general | solution.py:268
  212.0 0.0 reduce-scatter.2.cloned.1.call-update
  212.0 0.2 all-gather.7.cloned.1.call-start
  212.2 52.5 %reduce-scatter.2.cloned.1.call-done = bf16[256,2048]{1,0:T(8,128)(2,1)} async-done(((bf16[1024,2048]{1,0:T(8,128)(2,1)}), bf16[256,2048]{1,0:T(8,128)(2,1)}) %reduce-scatter.2.cloned.1.call-update) | async-done | bytes 1048592 | tf_op jit(solution)/shard_map/reduce_scatter | solution.py:267
  264.7 1.5 convert_element_type.48
  266.2 1.1 fusion.17
  267.3 0.0 all-gather.7.cloned.1.call-update
  267.3 35.3 %all-gather.7.cloned.1.call-done = bf16[1024,1024]{1,0:T(8,128)(2,1)} async-done(((bf16[256,1024]{1,0:T(8,128)(2,1)}), bf16[1024,1024]{1,0:T(8,128)(2,1)}) %all-gather.7.cloned.1.call-update) | async-done | bytes 2097168 | tf_op jit(solution)/shard_map/all_gather | solution.py:276
  302.6 0.0 copy-done
  302.6 5.3 %fusion.9 = bf16[1024,1024]{1,0:T(8,128)(2,1)} fusion(bf16[1024,1024]{1,0:T(8,128)(2,1)} %all-gather.7.cloned.1.call-done, bf16[1,1024,1024]{2,1,0:T(8,128)(2,1)S(1)} %copy-done), kind=kOutput, calls=%fused_computation.11 | convolution fusion | flops 2148532224 | bytes 6291456 | tf_op jit(solution)/shard_map/dot_general | solution.py:275
  307.9 0.0 copy-start.5
  307.9 5.7 %all-to-all-start.1 = ((bf16[8,128,1024]{2,1,0:T(8,128)(2,1)}), bf16[8,128,1024]{2,1,0:T(8,128)(2,1)}, u32[]{:S(2)}, u32[]{:S(2)}) async-start(bf16[8,128,1024]{2,1,0:T(8,128)(2,1)} %bitcast.30), calls=%async_computation.2 | async-start | bytes 4194304 | tf_op jit(solution)/shard_map/all_to_all | solution.py:280
  313.6 0.0 copy-done.5
  313.6 0.1 copy.20
  313.8 45.4 %all-to-all-done.1 = bf16[8,128,1024]{2,1,0:T(8,128)(2,1)} async-done(((bf16[8,128,1024]{2,1,0:T(8,128)(2,1)}), bf16[8,128,1024]{2,1,0:T(8,128)(2,1)}, u32[]{:S(2)}, u32[]{:S(2)}) %all-to-all-start.1) | async-done | bytes 2097184 | tf_op jit(solution)/shard_map/all_to_all | solution.py:280
  359.2 4.6 %gather_fusion.1 = bf16[512,1024]{1,0:T(8,128)(2,1)S(1)} fusion(bf16[1024,1024]{1,0:T(8,128)(2,1)} %bitcast.13, s32[1024]{0:T(1024)S(1)} %pad_clamp_fusion), kind=kCustom, calls=%fused_computation.1 | custom fusion | bytes 2099200 | tf_op jit(solution)/shard_map/gather | solution.py:288
  363.8 2.4 reshape.78
  366.1 0.0 copy-start.2
  366.1 4.3 %multiply_reduce_fusion = f32[256,1024]{1,0:T(8,128)S(1)} fusion(f32[256,2,1024]{2,1,0:T(2,128)} %reshape.78, f32[256,2]{1,0:T(8,128)S(1)} %copy.20), kind=kLoop, calls=%fused_computation.10 | loop fusion | flops 786432 | bytes 3147776 | tf_op jit(solution)/shard_map/reduce_sum | solution.py:292
  370.5 0.0 copy-done.2
  370.5 0.9 fusion.16
  (10 shorter events, 0.1 us)
Async XLA Ops:
  6.5 296.1 %copy-start = (bf16[1,1024,1024]{2,1,0:T(8,128)(2,1)S(1)}, bf16[1,1024,1024]{2,1,0:T(8,128)(2,1)}, u32[]{:S(2)}) copy-start(bf16[1,1024,1024]{2,1,0:T(8,128)(2,1)} %param.29) | copy-start | bytes 6291460
  6.5 73.6 %all-gather.9.cloned.1.call-start = ((), (), s32[]{:S(2)}) async-start(), calls=%async_computation.6 | async-start | bytes 2359296 | tf_op jit(solution)/shard_map/all_gather | solution.py:200
  49.3 83.5 %all-gather.5.cloned.1.call-start = ((), (), s32[]{:S(2)}) async-start(), calls=%async_computation.3 | async-start | bytes 2621440 | tf_op jit(solution)/shard_map/all_gather | solution.py:240
  80.2 11.9 %copy-start.3 = (s32[256,2]{0,1:T(2,128)S(1)}, s32[256,2]{0,1:T(2,128)}, u32[]{:S(2)}) copy-start(s32[256,2]{0,1:T(2,128)} %param.25) | copy-start | bytes 6148
  80.2 52.7 %copy-start.8 = (bf16[256,1024]{1,0:T(8,128)(2,1)S(1)}, bf16[256,1024]{1,0:T(8,128)(2,1)}, u32[]{:S(2)}) copy-start(bf16[256,1024]{1,0:T(8,128)(2,1)} %param.22) | copy-start | bytes 1572868
  92.0 172.7 %reduce-scatter.2.cloned.1.call-start = ((), (), s32[]{:S(2)}) async-start(), calls=%async_computation.4 | async-start | bytes 5242880 | tf_op jit(solution)/shard_map/reduce_scatter | solution.py:267
  96.8 49.5 %copy-start.4 = (f32[1024]{0:T(1024)S(1)}, f32[1024]{0:T(1024)}, u32[]{:S(2)}) copy-start(f32[1024]{0:T(1024)} %param.24) | copy-start | bytes 12292
  139.3 6.9 %copy-start.1 = (bf16[256,1024]{1,0:T(8,128)(2,1)}, bf16[256,1024]{1,0:T(8,128)(2,1)S(1)}, u32[]{:S(2)}) copy-start(bf16[256,1024]{1,0:T(8,128)(2,1)S(1)} %get-tuple-element.10) | copy-start | bytes 1572868
  151.9 53.9 %copy-start.6 = (bf16[1,1024,1024]{2,1,0:T(8,128)(2,1)S(1)}, bf16[1,1024,1024]{2,1,0:T(8,128)(2,1)}, u32[]{:S(2)}) copy-start(bf16[1,1024,1024]{2,1,0:T(8,128)(2,1)} %param.28) | copy-start | bytes 6291460
  151.9 53.9 %copy-start.7 = (bf16[1,1024,1024]{2,1,0:T(8,128)(2,1)S(1)}, bf16[1,1024,1024]{2,1,0:T(8,128)(2,1)}, u32[]{:S(2)}) copy-start(bf16[1,1024,1024]{2,1,0:T(8,128)(2,1)} %param.27) | copy-start | bytes 6291460
  212.0 90.6 %all-gather.7.cloned.1.call-start = ((), (), s32[]{:S(2)}) async-start(), calls=%async_computation.5 | async-start | bytes 2621440 | tf_op jit(solution)/shard_map/all_gather | solution.py:276
  307.9 5.7 %copy-start.5 = (f32[256,2]{0,1:T(2,128)S(1)}, f32[256,2]{0,1:T(2,128)}, u32[]{:S(2)}) copy-start(f32[256,2]{0,1:T(2,128)} %param.26) | copy-start | bytes 6148
  307.9 51.3 %all-to-all-start.1 = ((bf16[8,128,1024]{2,1,0:T(8,128)(2,1)}), bf16[8,128,1024]{2,1,0:T(8,128)(2,1)}, u32[]{:S(2)}, u32[]{:S(2)}) async-start(bf16[8,128,1024]{2,1,0:T(8,128)(2,1)} %bitcast.30), calls=%async_computation.2 | async-start | bytes 4194304 | tf_op jit(solution)/shard_map/all_to_all | solution.py:280
  366.1 4.3 %copy-start.2 = (bf16[256,1024]{1,0:T(8,128)(2,1)S(1)}, bf16[256,1024]{1,0:T(8,128)(2,1)}, u32[]{:S(2)}) copy-start(bf16[256,1024]{1,0:T(8,128)(2,1)} %copy-done.1) | copy-start | bytes 1572868
Sparse Core Ops, SparseCore 0:
  49.4 30.6 all-gather.8
  92.1 40.6 all-gather.4
  212.1 52.5 reduce-scatter.1
  267.4 35.1 all-gather.6

commit v2 on v1

--- a/solution.py
+++ b/solution.py
@@ -215,6 +215,88 @@
     )(place, reads, maps, gate_logits, group_gain.reshape(1, channels))
 
 
+def exchange(x, axis, shape, source, target, collective_id, name):
+    def kernel(x_ref, out_ref, stage, send_sem, recv_sem, local_sem):
+        n = lax.axis_size(axis)
+        me = lax.axis_index(axis)
+        peers = [lax.rem(me + step, n) for step in range(1, n)]
+        barrier = pltpu.get_barrier_semaphore()
+        for peer in peers:
+            pl.semaphore_signal(
+                barrier, inc=1, device_id={axis: peer}, device_id_type=pl.DeviceIdType.MESH
+            )
+        pl.semaphore_wait(barrier, n - 1)
+        copies = []
+        for step, peer in enumerate(peers):
+            copy = pltpu.make_async_remote_copy(
+                src_ref=source(x_ref, peer),
+                dst_ref=target(out_ref, me),
+                send_sem=send_sem.at[step],
+                recv_sem=recv_sem.at[step],
+                device_id={axis: peer},
+                device_id_type=pl.DeviceIdType.MESH,
+            )
+            copy.start()
+            copies.append(copy)
+        own = pltpu.make_async_copy(source(x_ref, me), stage, local_sem)
+        own.start()
+        own.wait()
+        own = pltpu.make_async_copy(stage, target(out_ref, me), local_sem)
+        own.start()
+        own.wait()
+        for copy in copies:
+            copy.wait()
+
+    n = lax.axis_size(axis)
+    return pl.pallas_call(
+        kernel,
+        in_specs=[pl.BlockSpec(memory_space=pl.ANY)],
+        out_specs=pl.BlockSpec(memory_space=pl.ANY),
+        out_shape=jax.ShapeDtypeStruct(shape, x.dtype),
+        scratch_shapes=[
+            pltpu.VMEM(x.shape[-2:], x.dtype),
+            pltpu.SemaphoreType.DMA((n - 1,)),
+            pltpu.SemaphoreType.DMA((n - 1,)),
+            pltpu.SemaphoreType.DMA,
+        ],
+        compiler_params=pltpu.CompilerParams(collective_id=collective_id, has_side_effects=True),
+        name=name,
+    )(x)
+
+
+def gather_columns(x, axis, collective_id):
+    rows, columns = x.shape
+    return exchange(
+        x,
+        axis,
+        (rows, lax.axis_size(axis) * columns),
+        lambda ref, peer: ref,
+        lambda ref, me: ref.at[:, pl.ds(pl.multiple_of(me * columns, columns), columns)],
+        collective_id,
+        "gather_columns",
+    )
+
+
+def gather_rows(x, axis, collective_id):
+    rows, columns = x.shape
+    return exchange(
+        x,
+        axis,
+        (lax.axis_size(axis) * rows, columns),
+        lambda ref, peer: ref,
+        lambda ref, me: ref.at[pl.ds(pl.multiple_of(me * rows, rows), rows), :],
+        collective_id,
+        "gather_rows",
+    )
+
+
+def swap_blocks(x, axis, collective_id):
+    return exchange(
+        x, axis, x.shape, lambda ref, peer: ref.at[peer], lambda ref, me: ref.at[me],
+        collective_id, "swap_blocks",
+    )
+
+
 def local(
     receptance,
     key_vectors,
@@ -237,7 +319,7 @@
     )
     tokens_here, features = residual.shape
     projected = jnp.dot(
-        lax.all_gather(mixed_rows, "tp", axis=1, tiled=True),
+        gather_columns(mixed_rows, "tp", 0),
         mixer_out,
         preferred_element_type=jnp.float32,
     )
@@ -261,7 +343,7 @@
     )
     padded = jnp.concatenate([normed, jnp.zeros((1, features), jnp.bfloat16)], axis=0)
     outgoing = padded[slot_table].reshape(experts_all, capacity, features)
-    arrived = lax.all_to_all(outgoing, "sp", split_axis=0, concat_axis=0, tiled=True)
+    arrived = swap_blocks(outgoing, "sp", 2)
     arrived_rows = arrived.reshape(-1, features)
     paired = jnp.concatenate([expert_gate[0], expert_up[0]], axis=1)
     gate_up = lax.psum_scatter(
@@ -273,16 +355,12 @@
     half_width = paired.shape[1] // 2
     hidden = (jax.nn.silu(gate_up[:, :half_width]) * gate_up[:, half_width:]).astype(jnp.bfloat16)
     expert_res = jnp.dot(
-        lax.all_gather(hidden, "tp", axis=0, tiled=True),
+        gather_rows(hidden, "tp", 1),
         expert_down[0],
         preferred_element_type=jnp.float32,
     )
-    returned = lax.all_to_all(
-        expert_res.astype(jnp.bfloat16).reshape(-1, capacity, features),
-        "sp",
-        split_axis=0,
-        concat_axis=0,
-        tiled=True,
+    returned = swap_blocks(
+        expert_res.astype(jnp.bfloat16).reshape(-1, capacity, features), "sp", 3
     )
     picked = (
         returned.reshape(-1, features)[slot_of]

time: 383 us -> 357 us (0.932); the launches traced: 378 us -> 357 us
  Pallas kernels: 54.6 us -> 211 us
  waiting for transfers between devices: 200 us -> 77.4 us
  blocking collectives: 60.8 us -> 7.79 us
  starting transfers between devices: 6.03 us -> 0.04 us
    pallas_call x0 -> x4, Pallas kernels: none -> 156 us  [exchange(): pl.pallas_call(kernel, in_specs=[pl.BlockSpec(memory_space=pl.ANY)], out_...]
    all_gather x2 -> x0, waiting for transfers between devices: 71.4 us -> none  [the longest x1 36 us: local(): lax.all_gather(mixed_rows, 'tp', axis=1, tiled=True)]
    all_to_all x1 -> x0, blocking collectives: 53.9 us -> none  [local(): lax.all_to_all(outgoing, 'sp', split_axis=0, concat_axis=0, tiled=True)]
    all_to_all x1 -> x0, waiting for transfers between devices: 45.4 us -> none  [local(): lax.all_to_all(expert_res.astype(jnp.bfloat16).reshape(-1, capacity, feat...]
    all_to_all x1 -> x0, starting transfers between devices: 5.72 us -> none  [local(): lax.all_to_all(expert_res.astype(jnp.bfloat16).reshape(-1, capacity, feat...]
    all_gather x1, waiting for transfers between devices: 30.8 us -> 26.1 us  [time_mix(): maps = lax.all_gather(states, 'sp')]
  transfers between devices with their start and end apart: 5 -> 2, of which waited for: 5 -> 2; matrix products, arithmetic and copies ran while one was open for 1% -> 1% of each run, Pallas kernels for 0% -> 0%
where the time goes in v2:
time: 357 us
  Pallas kernels  211 us (59%)
  waiting for transfers between devices  77.4 us (22%)
  matrix products  21 us (6%)
  local copies, waits for them, and re-layouts  16.5 us (5%)
  between operations  13.6 us (4%)
  other arithmetic  9.32 us (3%)
  blocking collectives  7.79 us (2%)
    pallas_call x4, Pallas kernels, exchange(): pl.pallas_call(kernel, in_specs=[pl.BlockSpec(memory_space=pl.ANY)], out_...  156 us
    reduce_scatter x1, waiting for transfers between devices, local(): lax.psum_scatter(jnp.dot(arrived_rows, paired, preferred_element_type=jnp...  51.3 us
    pallas_call x1, Pallas kernels, time_mix(): pl.pallas_call(mix_kernel, grid=(pairs,), in_specs=[wide] * 5, out_specs=...  42.8 us
    all_gather x1, waiting for transfers between devices, time_mix(): maps = lax.all_gather(states, 'sp')  26.1 us
    pallas_call x1, Pallas kernels, time_mix(): pl.pallas_call(read_kernel, grid=(pairs,), in_specs=[pl.BlockSpec(memory_...  11.8 us
    dot_general x1, matrix products, local(): jnp.dot(arrived_rows, paired, preferred_element_type=jnp.float32)  9.29 us
    psum x1, blocking collectives, local(): squares = lax.psum(jnp.sum(midway_f * midway_f, axis=1), 'tp')  7.79 us
  transfers between devices with their start and end apart: 2, of which 2 were waited for; matrix products, arithmetic and copies ran while one was open for 1% of the time, Pallas kernels for 0%

profile of v2, /device:TPU:9, one launch (start us, length us, event | category | flops | bytes accessed | tf_op | source)
XLA Modules:
  0.0 356.7 jit_solution(15476126800678838836)
XLA Ops:
  6.5 0.0 copy-start
  6.5 0.0 copy-start.3
  6.5 0.0 all-gather.3.cloned.1.call-start
  6.5 42.8 %mix.1 = (f32[256,2048]{1,0:T(8,128)}, bf16[1024,128]{1,0:T(8,128)(2,1)}) custom-call(bf16[256,1024]{1,0:T(8,128)(2,1)} %r_ref.1, bf16[256,1024]{1,0:T(8,128)(2,1)} %k_ref.1, bf16[256,1024]{1,0:T(8,128)(2,1)} %v_ref.1, bf16[256,1024]{1,0:T(8,128)(2,1)} %d_ref.1, bf16[256,1024]{1,0:T(8,128)(2,1)} %a_ref.1), custom_call_target="tpu_custom_call" | custom-call | tf_op jit(solution)/shard_map/mix/pallas_call | solution.py:189
  49.3 0.0 all-gather.3.cloned.1.call-update
  49.3 0.0 reduce-scatter.2.cloned.1.call-start
  49.4 0.0 copy-done.3
  49.4 0.1 copy.18
  49.5 0.1 eq.29
  49.7 0.1 eq.25
  49.8 1.1 reduce-window.6
  51.0 0.2 slice_reduce_fusion
  51.2 0.1 copy.17
  51.4 0.1 mul.60
  51.6 0.1 fusion.19
  51.6 2.4 scatter_custom_fusion
  54.1 26.1 %all-gather.3.cloned.1.call-done = bf16[8192,128]{1,0:T(8,128)(2,1)} async-done(((bf16[1024,128]{1,0:T(8,128)(2,1)}), bf16[8192,128]{1,0:T(8,128)(2,1)}) %all-gather.3.cloned.1.call-update) | async-done | bytes 2097168 | tf_op jit(solution)/shard_map/all_gather | solution.py:200
  80.2 11.8 %read.1.x_ref = bf16[256,1024]{1,0:T(8,128)(2,1)} custom-call(s32[1]{0:T(128)} %bitcast.place_ref, f32[256,2048]{1,0:T(8,128)} %get-tuple-element.7.read_ref, bf16[8,1024,128]{2,1,0:T(8,128)(2,1)} %bitcast.30, bf16[256,1024]{1,0:T(8,128)(2,1)} %gate_ref.1, f32[1,1024]{1,0:T(1,128)} %bitcast.36), custom_call_target="tpu_custom_call" | custom-call | tf_op jit(solution)/shard_map/read/pallas_call | solution.py:202
  92.0 0.0 copy-start.6
  92.0 25.4 %gather_columns.1 = bf16[256,4096]{1,0:T(8,128)(2,1)} custom-call(bf16[256,1024]{1,0:T(8,128)(2,1)} %read.1.x_ref), custom_call_target="tpu_custom_call" | custom-call | tf_op jit(solution)/shard_map/gather_columns/pallas_call | solution.py:251
  117.4 0.0 copy-done.6
  117.4 0.0 copy-start.4
  117.4 6.5 %fusion.15 = (f32[256]{0:T(256)S(1)}, bf16[256,1024]{1,0:T(8,128)(2,1)S(1)}) fusion(bf16[256,4096]{1,0:T(8,128)(2,1)} %gather_columns.1, bf16[4096,1024]{1,0:T(8,128)(2,1)} %param.23, bf16[256,1024]{1,0:T(8,128)(2,1)S(1)} %copy-done.6), kind=kOutput, calls=%fused_computation.19 | convolution fusion | flops 2149056256 | bytes 11535360 | tf_op jit(solution)/shard_map/dot_general | solution.py:321
  123.9 0.0 copy-start.1
  123.9 7.8 %psum.7 = f32[256]{0:T(256)S(1)} all-reduce(f32[256]{0:T(256)S(1)} %get-tuple-element.9), channel_id=1, replica_groups=mesh['sp'=8,'tp'=4] {'tp'}, use_global_device_ids=true, to_apply=%region_1.0 | all-reduce | flops 256 | bytes 2048 | tf_op jit(solution)/shard_map/psum | solution.py:328
  131.7 0.0 copy-done.1
  131.7 0.0 copy-done.4
  131.7 0.2 fusion.14
  131.9 5.4 %gather_fusion = bf16[1024,1024]{1,0:T(8,128)(2,1)} fusion(bf16[257,1024]{1,0:T(8,128)(2,1)S(1)} %concatenate.6, s32[1024]{0:T(1024)S(1)} %fusion.21), kind=kCustom, calls=%fused_computation | custom fusion | bytes 4198400 | tf_op jit(solution)/shard_map/gather | solution.py:345
  137.3 55.5 %swap_blocks.2 = bf16[8,128,1024]{2,1,0:T(8,128)(2,1)} custom-call(bf16[8,128,1024]{2,1,0:T(8,128)(2,1)} %bitcast.29), custom_call_target="tpu_custom_call" | custom-call | tf_op jit(solution)/shard_map/swap_blocks/pallas_call | solution.py:251
  192.8 9.3 %fusion.4 = bf16[1024,2048]{1,0:T(8,128)(2,1)} fusion(bf16[1024,1024]{1,0:T(8,128)(2,1)} %bitcast.31, bf16[1024,1024]{1,0:T(8,128)(2,1)} %bitcast.37, bf16[1024,1024]{1,0:T(8,128)(2,1)} %bitcast.38), kind=kOutput, calls=%fused_computation.7 | convolution fusion | flops 4305453056 | bytes 10485760 | tf_op jit(solution)/shard_map/dot_general | solution.py:350
  202.1 0.0 copy-start.5
  202.1 0.0 reduce-scatter.2.cloned.1.call-update
  202.2 0.7 copy-done.5
  202.8 0.1 copy.20
  203.0 51.3 %reduce-scatter.2.cloned.1.call-done = bf16[256,2048]{1,0:T(8,128)(2,1)} async-done(((bf16[1024,2048]{1,0:T(8,128)(2,1)}), bf16[256,2048]{1,0:T(8,128)(2,1)}) %reduce-scatter.2.cloned.1.call-update) | async-done | bytes 1048592 | tf_op jit(solution)/shard_map/reduce_scatter | solution.py:349
  254.2 1.5 convert_element_type.48
  255.7 1.1 fusion.17.x_ref
  256.8 26.4 %gather_rows.1 = bf16[1024,1024]{1,0:T(8,128)(2,1)} custom-call(bf16[256,1024]{1,0:T(8,128)(2,1)} %fusion.17.x_ref), custom_call_target="tpu_custom_call" | custom-call | tf_op jit(solution)/shard_map/gather_rows/pallas_call | solution.py:251
  283.2 0.0 copy-done
  283.2 5.3 %fusion.9 = bf16[1024,1024]{1,0:T(8,128)(2,1)} fusion(bf16[1024,1024]{1,0:T(8,128)(2,1)} %gather_rows.1, bf16[1,1024,1024]{2,1,0:T(8,128)(2,1)S(1)} %copy-done), kind=kOutput, calls=%fused_computation.11 | convolution fusion | flops 2148532224 | bytes 6291456 | tf_op jit(solution)/shard_map/dot_general | solution.py:357
  288.5 49.2 %swap_blocks.3 = bf16[8,128,1024]{2,1,0:T(8,128)(2,1)} custom-call(bf16[8,128,1024]{2,1,0:T(8,128)(2,1)} %bitcast.32), custom_call_target="tpu_custom_call" | custom-call | tf_op jit(solution)/shard_map/swap_blocks/pallas_call | solution.py:251
  337.6 4.6 %gather_fusion.1 = bf16[512,1024]{1,0:T(8,128)(2,1)S(1)} fusion(bf16[1024,1024]{1,0:T(8,128)(2,1)} %bitcast.28, s32[1024]{0:T(1024)S(1)} %pad_clamp_fusion), kind=kCustom, calls=%fused_computation.1 | custom fusion | bytes 2099200 | tf_op jit(solution)/shard_map/gather | solution.py:366
  342.2 2.4 reshape.78
  344.6 0.0 copy-start.2
  344.6 4.3 %multiply_reduce_fusion = f32[256,1024]{1,0:T(8,128)S(1)} fusion(f32[256,2,1024]{2,1,0:T(2,128)} %reshape.78, f32[256,2]{1,0:T(8,128)S(1)} %copy.20), kind=kLoop, calls=%fused_computation.10 | loop fusion | flops 786432 | bytes 3147776 | tf_op jit(solution)/shard_map/reduce_sum | solution.py:370
  349.0 0.0 copy-done.2
  349.0 0.9 fusion.16
  (10 shorter events, 0.1 us)
Async XLA Ops:
  6.5 276.6 %copy-start = (bf16[1,1024,1024]{2,1,0:T(8,128)(2,1)S(1)}, bf16[1,1024,1024]{2,1,0:T(8,128)(2,1)}, u32[]{:S(2)}) copy-start(bf16[1,1024,1024]{2,1,0:T(8,128)(2,1)} %param.29) | copy-start | bytes 6291460
  6.5 42.8 %copy-start.3 = (s32[256,2]{0,1:T(2,128)S(1)}, s32[256,2]{0,1:T(2,128)}, u32[]{:S(2)}) copy-start(s32[256,2]{0,1:T(2,128)} %param.25) | copy-start | bytes 6148
  6.5 73.7 %all-gather.3.cloned.1.call-start = ((), (), s32[]{:S(2)}) async-start(), calls=%async_computation.2 | async-start | bytes 2359296 | tf_op jit(solution)/shard_map/all_gather | solution.py:200
  49.3 204.9 %reduce-scatter.2.cloned.1.call-start = ((), (), s32[]{:S(2)}) async-start(), calls=%async_computation.1 | async-start | bytes 5242880 | tf_op jit(solution)/shard_map/reduce_scatter | solution.py:349
  92.0 25.4 %copy-start.6 = (bf16[256,1024]{1,0:T(8,128)(2,1)S(1)}, bf16[256,1024]{1,0:T(8,128)(2,1)}, u32[]{:S(2)}) copy-start(bf16[256,1024]{1,0:T(8,128)(2,1)} %param.22) | copy-start | bytes 1572868
  117.4 14.3 %copy-start.4 = (f32[1024]{0:T(1024)S(1)}, f32[1024]{0:T(1024)}, u32[]{:S(2)}) copy-start(f32[1024]{0:T(1024)} %param.24) | copy-start | bytes 12292
  123.9 7.8 %copy-start.1 = (bf16[256,1024]{1,0:T(8,128)(2,1)}, bf16[256,1024]{1,0:T(8,128)(2,1)S(1)}, u32[]{:S(2)}) copy-start(bf16[256,1024]{1,0:T(8,128)(2,1)S(1)} %get-tuple-element.10) | copy-start | bytes 1572868
  202.1 0.7 copy-start.5
  344.6 4.3 %copy-start.2 = (bf16[256,1024]{1,0:T(8,128)(2,1)S(1)}, bf16[256,1024]{1,0:T(8,128)(2,1)}, u32[]{:S(2)}) copy-start(bf16[256,1024]{1,0:T(8,128)(2,1)} %copy-done.1) | copy-start | bytes 1572868
Sparse Core Ops, SparseCore 0:
  49.4 30.7 all-gather.2
  202.3 51.9 reduce-scatter.1
